TPU v7x, 32 devices: a whole 2x2x4 slice. The times are simulated.
32 devices in a mesh: fs: 4 (over y, x), tp: 8 (over z, core).
Axes of the slice: x: 2, y: 2, z: 4, core: 2. Of those that a mesh axis runs over, the one named last changes fastest.
Arguments:
- normed_inputs: bfloat16 [4096, 4096], P('fs', 'tp'), may hold values from -6 to 6
- query_upstream: bfloat16 [4096, 4096], P('fs', 'tp'), may hold values from -0.125 to 0.125
- key_upstream: bfloat16 [4096, 1024], P('fs', 'tp'), may hold values from -0.09375 to 0.09375
- head_outputs: bfloat16 [4096, 4096], P('fs', 'tp'), may hold values from -6 to 6
- branch_upstream: bfloat16 [4096, 4096], P('fs', 'tp'), may hold values from -0.125 to 0.125
- query_master: float32 [4096, 4096], P('fs', 'tp'), may hold values from -0.09375 to 0.09375
- key_master: float32 [4096, 1024], P('fs', 'tp'), may hold values from -0.09375 to 0.09375
- branch_master: float32 [4096, 4096], P('fs', 'tp'), may hold values from -0.09375 to 0.09375
- query_basis: bfloat16 [4096, 128], replicated, may hold values from -0.09375 to 0.09375
- key_basis: bfloat16 [4096, 128], replicated, may hold values from -0.09375 to 0.09375
- branch_basis: bfloat16 [4096, 128], replicated, may hold values from -0.09375 to 0.09375
- query_first: float32 [128, 4096], P(None, 'tp'), may hold values from -0.75 to 0.75
- query_second: float32 [128, 4096], P(None, 'tp'), may hold values from 0.001 to 0.02
- key_first: float32 [128, 1024], P(None, 'tp'), may hold values from -0.75 to 0.75
- key_second: float32 [128, 1024], P(None, 'tp'), may hold values from 0.001 to 0.02
- branch_first: float32 [4096, 128], P('fs'), may hold values from -0.75 to 0.75
- branch_second: float32 [4096, 128], P('fs'), may hold values from 0.001 to 0.02
Outputs:
- query_step: float32 [4096, 4096], P('fs', 'tp')
- key_step: float32 [4096, 1024], P('fs', 'tp')
- branch_step: float32 [4096, 4096], P('fs', 'tp')
- query_updated: float32 [4096, 4096], P('fs', 'tp')
- key_updated: float32 [4096, 1024], P('fs', 'tp')
- branch_updated: float32 [4096, 4096], P('fs', 'tp')
- query_copy: bfloat16 [4096, 4096], P(None, 'tp')
- key_copy: bfloat16 [4096, 1024], P(None, 'tp')
- branch_copy: bfloat16 [4096, 4096], P(None, 'tp')
- query_first_new: float32 [128, 4096], P(None, 'tp')
- query_second_new: float32 [128, 4096], P(None, 'tp')
- key_first_new: float32 [128, 1024], P(None, 'tp')
- key_second_new: float32 [128, 1024], P(None, 'tp')
- branch_first_new: float32 [4096, 128], P('fs')
- branch_second_new: float32 [4096, 128], P('fs')
All inputs are finite; a program needn't handle non-finite values.
Results may differ from a plain program's by a relative error of at most 0.001.
Values may be sent and summed in bfloat16 or wider, within the bound.
No kernel may reach another device: no remote copies, remote signals or barrier semaphores. Data moves between devices by JAX's collectives and lax.ppermute only.
A program may use at most 128 MiB of HBM per device.

v0:
```python
import jax
import jax.numpy as jnp
from jax import lax
from jax.sharding import PartitionSpec as P

LEARN = 0.02
BETA_ONE = 0.9
BETA_TWO = 0.95
ADAM_EPS = 1e-08
CLIP_RMS = 0.5


def moments(first, second, low, clip):
    scaled = clip * low
    first_new = BETA_ONE * first + (1.0 - BETA_ONE) * scaled
    second_new = BETA_TWO * second + (1.0 - BETA_TWO) * scaled * scaled
    return (first_new, second_new, first_new / (jnp.sqrt(second_new) + ADAM_EPS))


def over_tokens(left, right, precision=None):
    return lax.dot_general(
        left,
        right,
        (((0,), (0,)), ((), ())),
        precision=precision,
        preferred_element_type=jnp.float32,
    )


def per_device(
    normed_inputs,
    query_upstream,
    key_upstream,
    head_outputs,
    branch_upstream,
    query_master,
    key_master,
    branch_master,
    query_basis,
    key_basis,
    branch_basis,
    query_first,
    query_second,
    key_first,
    key_second,
    branch_first,
    branch_second,
):
    exact = lax.Precision.HIGHEST
    row_index = lax.axis_index("fs")
    col_index = lax.axis_index("tp")
    n_rows = lax.axis_size("fs")
    n_cols = lax.axis_size("tp")
    features = normed_inputs.shape[1]
    query_local = query_upstream.shape[1]
    key_local = key_upstream.shape[1]
    rows_in = query_master.shape[0]
    rank = query_basis.shape[1]
    whole_values = lax.all_gather(head_outputs, "tp", axis=1, tiled=True)
    block_query = lax.dynamic_slice_in_dim(query_basis, col_index * features, features, 0)
    block_key = lax.dynamic_slice_in_dim(key_basis, col_index * features, features, 0)
    proj_query, proj_key = lax.psum(
        (
            jnp.dot(normed_inputs, block_query, preferred_element_type=jnp.float32),
            jnp.dot(normed_inputs, block_key, preferred_element_type=jnp.float32),
        ),
        "tp",
    )
    part_query = over_tokens(proj_query, query_upstream.astype(jnp.float32), exact)
    part_key = over_tokens(proj_key, key_upstream.astype(jnp.float32), exact)
    grad_branch = lax.psum_scatter(
        over_tokens(whole_values, branch_upstream), "fs", scatter_dimension=0, tiled=True
    )
    own_branch = lax.dynamic_slice_in_dim(branch_basis, col_index * features, features, 0).astype(
        jnp.float32
    )
    part_branch = jnp.dot(grad_branch, own_branch, precision=exact)
    query_low, key_low = lax.psum((part_query, part_key), "fs")
    branch_low = lax.psum(part_branch, "tp")
    local_squares = (jnp.sum(query_low * query_low) + jnp.sum(key_low * key_low)) / n_rows
    local_squares = local_squares + jnp.sum(branch_low * branch_low) / n_cols
    total = lax.psum(local_squares, ("fs", "tp"))
    entries = rank * n_cols * (2 * query_local + key_local)
    rms_value = jnp.sqrt(total / float(entries))
    clip = 1.0 / jnp.maximum(1.0, rms_value / CLIP_RMS)
    q_first, q_second, q_dir = moments(query_first, query_second, query_low, clip)
    k_first, k_second, k_dir = moments(key_first, key_second, key_low, clip)
    b_first, b_second, b_dir = moments(branch_first, branch_second, branch_low, clip)
    step_rows_query = lax.dynamic_slice_in_dim(query_basis, row_index * rows_in, rows_in, 0).astype(
        jnp.float32
    )
    step_rows_key = lax.dynamic_slice_in_dim(key_basis, row_index * rows_in, rows_in, 0).astype(
        jnp.float32
    )
    query_step = jnp.dot(step_rows_query, q_dir, precision=exact)
    key_step = jnp.dot(step_rows_key, k_dir, precision=exact)
    branch_step = jnp.dot(b_dir, own_branch.T, precision=exact)
    query_updated = query_master - LEARN * query_step
    key_updated = key_master - LEARN * key_step
    branch_updated = branch_master - LEARN * branch_step
    query_copy, key_copy, branch_copy = (
        lax.all_gather(query_updated.astype(jnp.bfloat16), "fs", axis=0, tiled=True),
        lax.all_gather(key_updated.astype(jnp.bfloat16), "fs", axis=0, tiled=True),
        lax.all_gather(branch_updated.astype(jnp.bfloat16), "fs", axis=0, tiled=True),
    )
    return (
        query_step,
        key_step,
        branch_step,
        query_updated,
        key_updated,
        branch_updated,
        query_copy,
        key_copy,
        branch_copy,
        q_first,
        q_second,
        k_first,
        k_second,
        b_first,
        b_second,
    )


def solution(mesh):
    return jax.shard_map(
        per_device,
        mesh=mesh,
        in_specs=(
            P("fs", "tp"),
            P("fs", "tp"),
            P("fs", "tp"),
            P("fs", "tp"),
            P("fs", "tp"),
            P("fs", "tp"),
            P("fs", "tp"),
            P("fs", "tp"),
            P(),
            P(),
            P(),
            P(None, "tp"),
            P(None, "tp"),
            P(None, "tp"),
            P(None, "tp"),
            P("fs", None),
            P("fs", None),
        ),
        out_specs=(
            P("fs", "tp"),
            P("fs", "tp"),
            P("fs", "tp"),
            P("fs", "tp"),
            P("fs", "tp"),
            P("fs", "tp"),
            P(None, "tp"),
            P(None, "tp"),
            P(None, "tp"),
            P(None, "tp"),
            P(None, "tp"),
            P(None, "tp"),
            P(None, "tp"),
            P("fs", None),
            P("fs", None),
        ),
        check_vma=False,
    )
```

profile of v0, /device:TPU:0, one launch (start us, length us, event | category | flops | bytes accessed | tf_op | source)
XLA Modules:
  0.0 502.3 jit_solution(1356573704103843505)
XLA Ops:
  8.0 86.4 %all-gather.5.cloned.1.call-done = bf16[1024,4096]{1,0:T(8,128)(2,1)} async-done(((bf16[1024,512]{1,0:T(8,128)(2,1)}), bf16[1024,4096]{1,0:T(8,128)(2,1)}) %all-gather.5.cloned.1.call-update) | async-done | bytes 8388624 | tf_op jit(solution)/shard_map/all_gather | solution.py:59
  94.4 10.4 %fusion.39 = f32[4096,512]{1,0:T(8,128)} fusion(bf16[1024,4096]{1,0:T(8,128)(2,1)} %all-gather.5.cloned.1.call-done, bf16[1024,512]{1,0:T(8,128)(2,1)S(1)} %copy-done), kind=kOutput, calls=%fused_computation.53 | convolution fusion | flops 4294967296 | bytes 17825792 | tf_op jit(solution)/shard_map/dot_general | solution.py:21
  104.9 1.1 copy-done.2
  106.1 2.2 convolution_bitcast_fusion
  108.2 2.2 convolution_bitcast_fusion.1
  110.4 79.4 %reduce-scatter.2.cloned.1.call-done = f32[1024,512]{1,0:T(8,128)} async-done(((f32[4096,512]{1,0:T(8,128)}), f32[1024,512]{1,0:T(8,128)}) %reduce-scatter.2.cloned.1.call-update) | async-done | bytes 2097168 | tf_op jit(solution)/shard_map/reduce_scatter | solution.py:71
  189.8 3.4 fusion.18
  193.4 62.4 %all-reduce.5.cloned.1.call-done = (f32[1024,128]{0,1:T(8,128)}, f32[1024,128]{0,1:T(8,128)}, f32[1024,128]{1,0:T(8,128)}) async-done(((f32[1024,128]{0,1:T(8,128)}, f32[1024,128]{0,1:T(8,128)}, f32[1024,128]{1,0:T(8,128)}), (f32[1024,128]{0,1:T(8,128)}, f32[1024,128]{0,1:T(8,128)}, f32[1024,128]{1,0:T(8,128)})) %all-reduce.5.cloned.1.call-update) | async-done | bytes 1572880 | tf_op jit(solution)/shard_map/psum | solution.py:62
  255.8 2.5 fusion.37
  258.3 1.0 fusion.38
  260.7 41.6 %all-reduce.7.cloned.1.call-done = (f32[128,512]{1,0:T(8,128)}, f32[128,128]{1,0:T(8,128)}) async-done(((f32[128,512]{1,0:T(8,128)}, f32[128,128]{1,0:T(8,128)}), (f32[128,512]{1,0:T(8,128)}, f32[128,128]{1,0:T(8,128)})) %all-reduce.7.cloned.1.call-update) | async-done | bytes 327696 | tf_op jit(solution)/shard_map/psum | solution.py:78
  302.3 1.6 multiply_reduce_fusion.1
  303.9 1.5 multiply_reduce_fusion.2
  306.7 39.3 %psum.47 = f32[]{:T(128)} all-reduce(f32[]{:T(128)S(6)} %add.68), channel_id=1, replica_groups=mesh['fs'=4,'tp'=8] {'fs','tp'}, use_global_device_ids=true, to_apply=%region_9.0 | all-reduce | flops 1 | bytes 8 | tf_op jit(solution)/shard_map/psum | solution.py:82
  347.7 2.6 fusion.35
  350.3 1.4 fusion
  351.7 4.7 fusion.34
  356.5 1.2 fusion.5
  358.1 4.5 fusion.36
  362.7 15.2 %all-gather.9.cloned.1.call-done = bf16[4096,128]{1,0:T(8,128)(2,1)} async-done(((bf16[1024,128]{1,0:T(8,128)(2,1)}), bf16[4096,128]{1,0:T(8,128)(2,1)}) %all-gather.9.cloned.1.call-update) | async-done | bytes 1048592 | tf_op jit(solution)/shard_map/all_gather | solution.py:103
  377.9 54.9 %all-gather.11.cloned.1.call-done = bf16[4096,512]{1,0:T(8,128)(2,1)} async-done(((bf16[1024,512]{1,0:T(8,128)(2,1)}), bf16[4096,512]{1,0:T(8,128)(2,1)}) %all-gather.11.cloned.1.call-update) | async-done | bytes 4194320 | tf_op jit(solution)/shard_map/all_gather | solution.py:104
  432.8 55.0 %all-gather.7.cloned.1.call-done = bf16[4096,512]{1,0:T(8,128)(2,1)} async-done(((bf16[1024,512]{1,0:T(8,128)(2,1)}), bf16[4096,512]{1,0:T(8,128)(2,1)}) %all-gather.7.cloned.1.call-update) | async-done | bytes 4194320 | tf_op jit(solution)/shard_map/all_gather | solution.py:102
  487.8 4.6 copy.40
  493.4 2.0 copy.42
  (60 shorter events, 4.2 us)
Async XLA Ops:
  7.2 87.2 %copy-start = (bf16[1024,512]{1,0:T(8,128)(2,1)S(1)}, bf16[1024,512]{1,0:T(8,128)(2,1)}, u32[]{:S(2)}) copy-start(bf16[1024,512]{1,0:T(8,128)(2,1)} %param.21) | copy-start | bytes 3145732
  7.2 87.2 %all-gather.5.cloned.1.call-start = ((), (), s32[]{:S(2)}) async-start(), calls=%async_computation.1 | async-start | bytes 9437184 | tf_op jit(solution)/shard_map/all_gather | solution.py:59
  7.9 181.9 %reduce-scatter.2.cloned.1.call-start = ((), (), s32[]{:S(2)}) async-start(), calls=%async_computation.2 | async-start | bytes 10485760 | tf_op jit(solution)/shard_map/reduce_scatter | solution.py:71
  104.9 150.9 %all-reduce.5.cloned.1.call-start = ((), (), s32[]{:S(2)}) async-start(), calls=%async_computation.6 | async-start | bytes 3145728 | tf_op jit(solution)/shard_map/psum | solution.py:62
  110.4 145.4 %copy-start.11 = (bf16[1024,512]{1,0:T(8,128)(2,1)S(1)}, bf16[1024,512]{1,0:T(8,128)(2,1)}, u32[]{:S(2)}) copy-start(bf16[1024,512]{1,0:T(8,128)(2,1)} %param.18) | copy-start | bytes 3145732
  193.3 65.0 %copy-start.19 = (bf16[1024,128]{1,0:T(8,128)(2,1)S(1)}, bf16[1024,128]{1,0:T(8,128)(2,1)}, u32[]{:S(2)}) copy-start(bf16[1024,128]{1,0:T(8,128)(2,1)} %param.19) | copy-start | bytes 786436
  193.3 153.5 %copy-start.20 = (f32[128,128]{1,0:T(8,128)S(1)}, f32[128,128]{1,0:T(8,128)}, u32[]{:S(2)}) copy-start(f32[128,128]{1,0:T(8,128)} %param.31) | copy-start | bytes 196612
  193.3 153.5 %copy-start.21 = (f32[128,128]{1,0:T(8,128)S(1)}, f32[128,128]{1,0:T(8,128)}, u32[]{:S(2)}) copy-start(f32[128,128]{1,0:T(8,128)} %param.30) | copy-start | bytes 196612
  193.3 109.0 %all-reduce.7.cloned.1.call-start = ((), (), s32[]{:S(2)}) async-start(), calls=%async_computation.7 | async-start | bytes 655360 | tf_op jit(solution)/shard_map/psum | solution.py:78
  255.8 91.9 %copy-start.14 = (f32[1024,128]{1,0:T(8,128)S(1)}, f32[1024,128]{1,0:T(8,128)}, u32[]{:S(2)}) copy-start(f32[1024,128]{1,0:T(8,128)} %param.23) | copy-start | bytes 1572868
  259.3 118.6 %all-gather.9.cloned.1.call-start = ((), (), s32[]{:S(2)}) async-start(), calls=%async_computation.4 | async-start | bytes 1310720 | tf_op jit(solution)/shard_map/all_gather | solution.py:103
  347.6 4.0 copy-start.17
  347.6 4.0 copy-start.18
  347.7 4.0 copy-start.7
  350.3 82.5 %all-gather.11.cloned.1.call-start = ((), (), s32[]{:S(2)}) async-start(), calls=%async_computation.5 | async-start | bytes 5242880 | tf_op jit(solution)/shard_map/all_gather | solution.py:104
  351.7 4.7 copy-start.4
  351.7 4.7 copy-start.5
  351.7 4.8 copy-start.12
  351.7 4.8 copy-start.16
  356.4 131.4 %all-gather.7.cloned.1.call-start = ((), (), s32[]{:S(2)}) async-start(), calls=%async_computation.3 | async-start | bytes 5242880 | tf_op jit(solution)/shard_map/all_gather | solution.py:102
  357.7 5.0 copy-start.9
  357.7 5.0 copy-start.10
  487.8 4.6 copy-start.13
  487.8 5.6 %copy-start.3 = (bf16[4096,512]{1,0:T(8,128)(2,1)S(1)}, bf16[4096,512]{1,0:T(8,128)(2,1)}, u32[]{:S(2)}) copy-start(bf16[4096,512]{1,0:T(8,128)(2,1)} %all-gather.11.cloned.1.call-done) | copy-start | bytes 12582916
  (5 other events, 11.0 us)
Sparse Core Ops, SparseCore 0:
  9.6 84.7 all-gather.4
  105.0 84.7 reduce-scatter.1
  193.6 62.1 all-reduce.4
  259.4 42.8 all-reduce.6
  350.4 27.4 all-gather.8
  380.2 52.5 all-gather.10
  435.2 52.5 all-gather.6
where the time goes:
time: 503 us; the launch traced here: 502 us
  waiting for transfers between devices  396 us (79%)
  blocking collectives  39.3 us (8%)
  matrix products  33.4 us (7%)
  between operations  17 us (3%)
  local copies, waits for them, and re-layouts  9.28 us (2%)
  other arithmetic  7.2 us (1%)
    all_gather x1, waiting for transfers between devices, per_device(): whole_values = lax.all_gather(head_outputs, 'tp', axis=1, tiled=True)  86.4 us
    reduce_scatter x1, waiting for transfers between devices, per_device(): lax.psum_scatter(over_tokens(whole_values, branch_upstream), 'fs', scatte...  79.4 us
    psum x1, waiting for transfers between devices, per_device(): lax.psum((jnp.dot(normed_inputs, block_query, preferred_element_type=jnp....  62.4 us
    all_gather x1, waiting for transfers between devices, per_device(): lax.all_gather(query_updated.astype(jnp.bfloat16), 'fs', axis=0, tiled=True)  55 us
    all_gather x1, waiting for transfers between devices, per_device(): lax.all_gather(branch_updated.astype(jnp.bfloat16), 'fs', axis=0, tiled=T...  54.9 us
    psum x1, waiting for transfers between devices, per_device(): query_low, key_low = lax.psum((part_query, part_key), 'fs')  41.6 us
    psum x1, blocking collectives, per_device(): total = lax.psum(local_squares, ('fs', 'tp'))  39.3 us
    all_gather x1, waiting for transfers between devices, per_device(): lax.all_gather(key_updated.astype(jnp.bfloat16), 'fs', axis=0, tiled=True)  15.2 us
  transfers between devices with their start and end apart: 7, of which 7 were waited for; matrix products, arithmetic and copies ran while one was open for 3% of the time, Pallas kernels for 0%

commit v1 on v0

--- a/solution.py
+++ b/solution.py
@@ -79,7 +79,7 @@
     branch_low = lax.psum(part_branch, "tp")
     local_squares = (jnp.sum(query_low * query_low) + jnp.sum(key_low * key_low)) / n_rows
     local_squares = local_squares + jnp.sum(branch_low * branch_low) / n_cols
-    total = lax.psum(local_squares, ("fs", "tp"))
+    total = jnp.sum(lax.all_gather(local_squares, ("fs", "tp")), axis=0)
     entries = rank * n_cols * (2 * query_local + key_local)
     rms_value = jnp.sqrt(total / float(entries))
     clip = 1.0 / jnp.maximum(1.0, rms_value / CLIP_RMS)

time: 503 us -> 503 us (level)
    psum x1 -> x0, blocking collectives: 39.3 us -> none  [per_device(): total = lax.psum(local_squares, ('fs', 'tp'))]
    unnamed x0 -> x1, blocking collectives: none -> 39.2 us
where the time goes in v1:
time: 503 us
  waiting for transfers between devices  396 us (79%)
  blocking collectives  39.2 us (8%)
  matrix products  33.4 us (7%)
  between operations  17.1 us (3%)
  local copies, waits for them, and re-layouts  9.42 us (2%)
  other arithmetic  7.82 us (2%)
    all_gather x1, waiting for transfers between devices, per_device(): whole_values = lax.all_gather(head_outputs, 'tp', axis=1, tiled=True)  86.4 us
    reduce_scatter x1, waiting for transfers between devices, per_device(): lax.psum_scatter(over_tokens(whole_values, branch_upstream), 'fs', scatte...  79.4 us
    psum x1, waiting for transfers between devices, per_device(): lax.psum((jnp.dot(normed_inputs, block_query, preferred_element_type=jnp....  62.4 us
    all_gather x1, waiting for transfers between devices, per_device(): lax.all_gather(query_updated.astype(jnp.bfloat16), 'fs', axis=0, tiled=True)  55 us
    all_gather x1, waiting for transfers between devices, per_device(): lax.all_gather(branch_updated.astype(jnp.bfloat16), 'fs', axis=0, tiled=T...  54.9 us
    psum x1, waiting for transfers between devices, per_device(): query_low, key_low = lax.psum((part_query, part_key), 'fs')  41.6 us
    unnamed x1, blocking collectives  39.2 us
    all_gather x1, waiting for transfers between devices, per_device(): lax.all_gather(key_updated.astype(jnp.bfloat16), 'fs', axis=0, tiled=True)  15 us
  transfers between devices with their start and end apart: 7, of which 7 were waited for; matrix products, arithmetic and copies ran while one was open for 3% of the time, Pallas kernels for 0%

profile of v1, /device:TPU:0, one launch (start us, length us, event | category | flops | bytes accessed | tf_op | source)
XLA Modules:
  0.0 502.8 jit_solution(8980494834195861181)
XLA Ops:
  8.0 86.4 %all-gather.5.cloned.1.call-done = bf16[1024,4096]{1,0:T(8,128)(2,1)} async-done(((bf16[1024,512]{1,0:T(8,128)(2,1)}), bf16[1024,4096]{1,0:T(8,128)(2,1)}) %all-gather.5.cloned.1.call-update) | async-done | bytes 8388624 | tf_op jit(solution)/shard_map/all_gather | solution.py:59
  94.4 10.5 %fusion.39 = f32[4096,512]{1,0:T(8,128)} fusion(bf16[1024,4096]{1,0:T(8,128)(2,1)} %all-gather.5.cloned.1.call-done, bf16[1024,512]{1,0:T(8,128)(2,1)S(1)} %copy-done), kind=kOutput, calls=%fused_computation.53 | convolution fusion | flops 4294967296 | bytes 17825792 | tf_op jit(solution)/shard_map/dot_general | solution.py:21
  104.9 1.1 copy-done.2
  106.1 2.2 convolution_bitcast_fusion
  108.3 2.2 convolution_bitcast_fusion.1
  110.4 79.4 %reduce-scatter.2.cloned.1.call-done = f32[1024,512]{1,0:T(8,128)} async-done(((f32[4096,512]{1,0:T(8,128)}), f32[1024,512]{1,0:T(8,128)}) %reduce-scatter.2.cloned.1.call-update) | async-done | bytes 2097168 | tf_op jit(solution)/shard_map/reduce_scatter | solution.py:71
  189.8 3.4 fusion.18
  193.4 62.4 %all-reduce.6.cloned.1.call-done = (f32[1024,128]{0,1:T(8,128)}, f32[1024,128]{0,1:T(8,128)}, f32[1024,128]{1,0:T(8,128)}) async-done(((f32[1024,128]{0,1:T(8,128)}, f32[1024,128]{0,1:T(8,128)}, f32[1024,128]{1,0:T(8,128)}), (f32[1024,128]{0,1:T(8,128)}, f32[1024,128]{0,1:T(8,128)}, f32[1024,128]{1,0:T(8,128)})) %all-reduce.6.cloned.1.call-update) | async-done | bytes 1572880 | tf_op jit(solution)/shard_map/psum | solution.py:62
  255.8 2.5 fusion.37
  258.3 1.0 fusion.38
  260.8 41.6 %all-reduce.8.cloned.1.call-done = (f32[128,512]{1,0:T(8,128)}, f32[128,128]{1,0:T(8,128)}) async-done(((f32[128,512]{1,0:T(8,128)}, f32[128,128]{1,0:T(8,128)}), (f32[128,512]{1,0:T(8,128)}, f32[128,128]{1,0:T(8,128)})) %all-reduce.8.cloned.1.call-update) | async-done | bytes 327696 | tf_op jit(solution)/shard_map/psum | solution.py:78
  302.3 1.6 multiply_reduce_fusion.1
  303.9 1.5 multiply_reduce_fusion.2
  306.8 39.2 %all-reduce = f32[32]{0:T(128)S(1)} all-reduce(f32[32]{0:T(128)S(1)} %dynamic-update-slice), channel_id=1, replica_groups=mesh['fs'=4,'tp'=8] {'fs','tp'}, use_global_device_ids=true, to_apply=%add | all-reduce | flops 32 | bytes 256
  348.4 2.6 fusion.35
  351.0 1.4 fusion
  352.4 4.7 fusion.34
  357.2 1.2 fusion.5
  358.8 4.5 fusion.36
  363.4 15.0 %all-gather.9.cloned.1.call-done = bf16[4096,128]{1,0:T(8,128)(2,1)} async-done(((bf16[1024,128]{1,0:T(8,128)(2,1)}), bf16[4096,128]{1,0:T(8,128)(2,1)}) %all-gather.9.cloned.1.call-update) | async-done | bytes 1048592 | tf_op jit(solution)/shard_map/all_gather | solution.py:103
  378.4 54.9 %all-gather.11.cloned.1.call-done = bf16[4096,512]{1,0:T(8,128)(2,1)} async-done(((bf16[1024,512]{1,0:T(8,128)(2,1)}), bf16[4096,512]{1,0:T(8,128)(2,1)}) %all-gather.11.cloned.1.call-update) | async-done | bytes 4194320 | tf_op jit(solution)/shard_map/all_gather | solution.py:104
  433.3 55.0 %all-gather.7.cloned.1.call-done = bf16[4096,512]{1,0:T(8,128)(2,1)} async-done(((bf16[1024,512]{1,0:T(8,128)(2,1)}), bf16[4096,512]{1,0:T(8,128)(2,1)}) %all-gather.7.cloned.1.call-update) | async-done | bytes 4194320 | tf_op jit(solution)/shard_map/all_gather | solution.py:102
  488.3 4.6 copy.41
  493.9 2.0 copy.43
  (63 shorter events, 4.9 us)
Async XLA Ops:
  7.2 87.2 %copy-start = (bf16[1024,512]{1,0:T(8,128)(2,1)S(1)}, bf16[1024,512]{1,0:T(8,128)(2,1)}, u32[]{:S(2)}) copy-start(bf16[1024,512]{1,0:T(8,128)(2,1)} %param.21) | copy-start | bytes 3145732
  7.2 87.2 %all-gather.5.cloned.1.call-start = ((), (), s32[]{:S(2)}) async-start(), calls=%async_computation.1 | async-start | bytes 9437184 | tf_op jit(solution)/shard_map/all_gather | solution.py:59
  7.9 181.9 %reduce-scatter.2.cloned.1.call-start = ((), (), s32[]{:S(2)}) async-start(), calls=%async_computation.2 | async-start | bytes 10485760 | tf_op jit(solution)/shard_map/reduce_scatter | solution.py:71
  104.9 150.9 %all-reduce.6.cloned.1.call-start = ((), (), s32[]{:S(2)}) async-start(), calls=%async_computation.6 | async-start | bytes 3145728 | tf_op jit(solution)/shard_map/psum | solution.py:62
  110.4 145.4 %copy-start.11 = (bf16[1024,512]{1,0:T(8,128)(2,1)S(1)}, bf16[1024,512]{1,0:T(8,128)(2,1)}, u32[]{:S(2)}) copy-start(bf16[1024,512]{1,0:T(8,128)(2,1)} %param.18) | copy-start | bytes 3145732
  193.3 65.0 %copy-start.19 = (bf16[1024,128]{1,0:T(8,128)(2,1)S(1)}, bf16[1024,128]{1,0:T(8,128)(2,1)}, u32[]{:S(2)}) copy-start(bf16[1024,128]{1,0:T(8,128)(2,1)} %param.19) | copy-start | bytes 786436
  193.3 154.1 %copy-start.20 = (f32[128,128]{1,0:T(8,128)S(1)}, f32[128,128]{1,0:T(8,128)}, u32[]{:S(2)}) copy-start(f32[128,128]{1,0:T(8,128)} %param.31) | copy-start | bytes 196612
  193.3 154.1 %copy-start.21 = (f32[128,128]{1,0:T(8,128)S(1)}, f32[128,128]{1,0:T(8,128)}, u32[]{:S(2)}) copy-start(f32[128,128]{1,0:T(8,128)} %param.30) | copy-start | bytes 196612
  193.3 109.0 %all-reduce.8.cloned.1.call-start = ((), (), s32[]{:S(2)}) async-start(), calls=%async_computation.7 | async-start | bytes 655360 | tf_op jit(solution)/shard_map/psum | solution.py:78
  255.8 92.5 %copy-start.14 = (f32[1024,128]{1,0:T(8,128)S(1)}, f32[1024,128]{1,0:T(8,128)}, u32[]{:S(2)}) copy-start(f32[1024,128]{1,0:T(8,128)} %param.23) | copy-start | bytes 1572868
  259.3 119.1 %all-gather.9.cloned.1.call-start = ((), (), s32[]{:S(2)}) async-start(), calls=%async_computation.4 | async-start | bytes 1310720 | tf_op jit(solution)/shard_map/all_gather | solution.py:103
  348.3 4.0 copy-start.17
  348.3 4.0 copy-start.18
  348.3 4.0 copy-start.7
  350.9 82.3 %all-gather.11.cloned.1.call-start = ((), (), s32[]{:S(2)}) async-start(), calls=%async_computation.5 | async-start | bytes 5242880 | tf_op jit(solution)/shard_map/all_gather | solution.py:104
  352.4 4.7 copy-start.4
  352.4 4.7 copy-start.5
  352.4 4.8 copy-start.12
  352.4 4.8 copy-start.16
  357.1 131.2 %all-gather.7.cloned.1.call-start = ((), (), s32[]{:S(2)}) async-start(), calls=%async_computation.3 | async-start | bytes 5242880 | tf_op jit(solution)/shard_map/all_gather | solution.py:102
  358.4 5.0 copy-start.9
  358.4 5.0 copy-start.10
  488.3 4.6 copy-start.13
  488.3 5.6 %copy-start.3 = (bf16[4096,512]{1,0:T(8,128)(2,1)S(1)}, bf16[4096,512]{1,0:T(8,128)(2,1)}, u32[]{:S(2)}) copy-start(bf16[4096,512]{1,0:T(8,128)(2,1)} %all-gather.11.cloned.1.call-done) | copy-start | bytes 12582916
  (5 other events, 11.0 us)
Sparse Core Ops, SparseCore 0:
  9.6 84.7 all-gather.4
  105.0 84.7 reduce-scatter.1
  193.6 62.1 all-reduce.5
  259.4 42.8 all-reduce.7
  351.1 27.3 all-gather.8
  380.7 52.5 all-gather.10
  435.7 52.5 all-gather.6
